TPU v7x, 32 devices: a whole 2x2x4 slice. The times are simulated.
32 devices in a mesh: sp: 8 (over z, x), tp: 4 (over y, core).
Axes of the slice: x: 2, y: 2, z: 4, core: 2. Of those that a mesh axis runs over, the one named last changes fastest.
Arguments:
- sequence_activations: bfloat16 [4096, 2048], P('sp', 'tp'), may hold values from -45 to 45
- entry_rescale_vector: float32 [2048], replicated, may hold values from 0.1 to 1.9
- blender_exit_switch_matrix: bfloat16 [2048, 2048], P('sp', 'tp'), may hold values from -0.125 to 0.125
- blender_entry_switch_matrix: bfloat16 [2048, 2048], P('sp', 'tp'), may hold values from -0.125 to 0.125
- blender_payload_matrix: bfloat16 [2048, 2048], P('sp', 'tp'), may hold values from -0.125 to 0.125
- scan_entry_matrix: bfloat16 [2048, 2048], P('sp', 'tp'), may hold values from -0.125 to 0.125
- scan_exit_switch_matrix: bfloat16 [2048, 2048], P('sp', 'tp'), may hold values from -0.125 to 0.125
- filter_blend_matrix: bfloat16 [2048, 2048], P('sp', 'tp'), may hold values from -0.125 to 0.125
- scan_blend_matrix: bfloat16 [2048, 2048], P('sp', 'tp'), may hold values from -0.125 to 0.125
- blender_kernel_coefficients: bfloat16 [3, 2048], P(None, 'tp'), may hold values from -3.5 to 3.5
- scan_kernel_coefficients: bfloat16 [4, 2048], P(None, 'tp'), may hold values from -3 to 3
- scan_switch_blockwise: bfloat16 [8, 256, 256], P('tp'), may hold values from -0.375 to 0.375
- entry_switch_blockwise: bfloat16 [8, 256, 256], P('tp'), may hold values from -0.375 to 0.375
- feature_fade_odds: float32 [2048], P('tp'), may hold values from 3 to 16
- fade_speed_multiplier: float32 [4096], P('sp'), may hold values from 0.3 to 2.8
- added_rate_shift: float32 [4096], P('sp'), may hold values from -1.4 to 0
- initial_hidden_vector: float32 [2048], P('tp'), may hold values from -6 to 6
- filter_exit_matrix: bfloat16 [2048, 2048], P('tp'), may hold values from -0.125 to 0.125
- scan_exit_matrix: bfloat16 [2048, 2048], P('tp'), may hold values from -0.125 to 0.125
Outputs:
- mixed: bfloat16 [4096, 2048], P('sp', 'tp')
All inputs are finite; a program needn't handle non-finite values.
Results may differ from a plain program's by a relative error of at most 0.015.
Values may be sent and summed in bfloat16 or wider, within the bound.
A program may use at most 64 MiB of HBM per device.

v0:
```python
import jax
import jax.numpy as jnp
from jax import lax
from jax.sharding import PartitionSpec as P

scan_switch_exponent = 8.0
norm_eps = 1e-06


def passed_along(value, axis, by):
    peers = lax.axis_size(axis)
    pairs = [(i, i + by) for i in range(peers) if 0 <= i + by < peers]
    return lax.ppermute(value, axis, pairs)


def entering(value, axis, combine, identity):
    peers, place = (lax.axis_size(axis), lax.axis_index(axis))
    everything = jax.tree.map(lambda part: lax.all_gather(part, axis), value)
    start = jax.tree.map(
        lambda part, zero: jnp.broadcast_to(jnp.asarray(zero, part.dtype), part.shape),
        value,
        identity,
    )

    def step(k, before):
        reached = k < place
        new = combine(before, jax.tree.map(lambda part: part[k], everything))
        return jax.tree.map(lambda a, b: jnp.where(reached, a, b), new, before)

    return lax.fori_loop(0, peers, step, start)


def linear_chain(earlier, later):
    return (earlier[0] * later[0], later[0] * earlier[1] + later[1])


def causal_local(previous, values, weights):
    taps = weights.shape[0]
    length = values.shape[0]
    extended = jnp.concatenate([previous, values], axis=0)
    result = extended[0:length] * weights[0].astype(jnp.float32)
    for tap_index in range(1, taps):
        result = result + extended[tap_index : tap_index + length] * weights[tap_index].astype(
            jnp.float32
        )
    return result


def local(
    sequence_activations,
    entry_rescale_vector,
    blender_exit_switch_matrix,
    blender_entry_switch_matrix,
    blender_payload_matrix,
    scan_entry_matrix,
    scan_exit_switch_matrix,
    filter_blend_matrix,
    scan_blend_matrix,
    blender_kernel_coefficients,
    scan_kernel_coefficients,
    scan_switch_blockwise,
    entry_switch_blockwise,
    feature_fade_odds,
    fade_speed_multiplier,
    added_rate_shift,
    initial_hidden_vector,
    filter_exit_matrix,
    scan_exit_matrix,
):
    row_count = sequence_activations.shape[0]
    feature_count = entry_rescale_vector.shape[0]
    pieces = [
        blender_exit_switch_matrix,
        blender_entry_switch_matrix,
        blender_payload_matrix,
        scan_entry_matrix,
        scan_exit_switch_matrix,
        filter_blend_matrix,
        scan_blend_matrix,
    ]
    local_cat = jnp.concatenate(pieces, axis=1)
    whole_weight = lax.all_gather(local_cat, "sp", axis=0, tiled=True)
    piece = lax.all_gather(sequence_activations, "tp", axis=1, tiled=True)
    piece_float = piece.astype(jnp.float32)
    scaled_piece = (piece.astype(jnp.float32) * entry_rescale_vector[None, :]).astype(jnp.bfloat16)
    totals = jnp.dot(scaled_piece, whole_weight, preferred_element_type=jnp.float32)
    squares = jnp.sum(piece_float * piece_float, axis=1)
    inverse = lax.rsqrt(squares / feature_count + norm_eps)
    projected = (totals * inverse[:, None]).astype(jnp.bfloat16)
    outputs = []
    offset = 0
    for weight in pieces:
        outputs.append(projected[:, offset : offset + weight.shape[1]])
        offset = offset + weight.shape[1]
    conv_b, conv_c, conv_x, lru_in, lru_gate, mix_conv, mix_lru = outputs
    short_in = conv_c.astype(jnp.float32) * conv_x.astype(jnp.float32)
    lru_float = lru_in.astype(jnp.float32)
    short_edge = blender_kernel_coefficients.shape[0] - 1
    lru_edge = scan_kernel_coefficients.shape[0] - 1
    prev_short, prev_lru = passed_along(
        (short_in[row_count - short_edge :], lru_float[row_count - lru_edge :]), "sp", 1
    )
    lru_conv = causal_local(prev_lru, lru_float, scan_kernel_coefficients).astype(jnp.bfloat16)
    head_local = scan_switch_blockwise.shape[0]
    head_size = scan_switch_blockwise.shape[1]
    lru_local = lru_conv.shape[1]
    heads = lru_conv.reshape(row_count, head_local, head_size)
    scan_switch_amount = jax.nn.sigmoid(
        jnp.einsum("thi,hij->thj", heads, scan_switch_blockwise, preferred_element_type=jnp.float32)
    ).reshape(row_count, lru_local)
    gate_i = jax.nn.sigmoid(
        jnp.einsum(
            "thi,hij->thj", heads, entry_switch_blockwise, preferred_element_type=jnp.float32
        )
    ).reshape(row_count, lru_local)
    position = lax.axis_index("sp") * row_count + jnp.arange(row_count, dtype=jnp.int32)
    fade_exponent_multiplier = (
        scan_switch_exponent
        * scan_switch_amount
        * jax.nn.log_sigmoid(feature_fade_odds)[None, :]
        * fade_speed_multiplier[:, None]
        + added_rate_shift[:, None]
    )
    decay = jnp.exp(fade_exponent_multiplier)
    scale = jnp.sqrt(-jnp.expm1(2.0 * fade_exponent_multiplier))
    scale = jnp.where((position == 0)[:, None], jnp.float32(1.0), scale)
    drive = scale * gate_i * lru_conv.astype(jnp.float32)
    cum_decay, cum_drive = lax.associative_scan(linear_chain, (decay, drive), axis=0)
    ones_state = jnp.ones((lru_local,), jnp.float32)
    zero_state = jnp.zeros((lru_local,), jnp.float32)
    pref_decay, pref_state = entering(
        (cum_decay[-1], cum_drive[-1]), "sp", linear_chain, (ones_state, zero_state)
    )
    carry_in = pref_decay * initial_hidden_vector + pref_state
    state = cum_drive + cum_decay * carry_in[None, :]
    lru_mix = (state * jax.nn.gelu(lru_gate.astype(jnp.float32), approximate=True)).astype(
        jnp.bfloat16
    )
    conv_mix = (
        conv_b.astype(jnp.float32) * causal_local(prev_short, short_in, blender_kernel_coefficients)
    ).astype(jnp.bfloat16)
    conv_part = jnp.dot(conv_mix, filter_exit_matrix, preferred_element_type=jnp.float32)
    lru_part = jnp.dot(lru_mix, scan_exit_matrix, preferred_element_type=jnp.float32)
    conv_sum, lru_sum = (
        lax.psum_scatter(
            conv_part.astype(jnp.bfloat16), "tp", scatter_dimension=1, tiled=True
        ).astype(jnp.float32),
        lax.psum_scatter(
            lru_part.astype(jnp.bfloat16), "tp", scatter_dimension=1, tiled=True
        ).astype(jnp.float32),
    )
    mixed = (
        jax.nn.sigmoid(mix_conv.astype(jnp.float32)) * conv_sum
        + jax.nn.sigmoid(mix_lru.astype(jnp.float32)) * lru_sum
    )
    return mixed.astype(jnp.bfloat16)


def solution(mesh):
    placed = (
        P("sp", "tp"),
        P(),
        P("sp", "tp"),
        P("sp", "tp"),
        P("sp", "tp"),
        P("sp", "tp"),
        P("sp", "tp"),
        P("sp", "tp"),
        P("sp", "tp"),
        P(None, "tp"),
        P(None, "tp"),
        P("tp", None, None),
        P("tp", None, None),
        P("tp"),
        P("sp"),
        P("sp"),
        P("tp"),
        P("tp", None),
        P("tp", None),
    )
    return jax.shard_map(
        local, mesh=mesh, in_specs=placed, out_specs=P("sp", "tp"), check_vma=False
    )
```

profile of v0, /device:TPU:0, one launch (start us, length us, event | category | flops | bytes accessed | tf_op | source)
XLA Modules:
  0.0 475.5 jit_solution(15577859545988110399)
XLA Ops:
  7.3 1.7 constant_dynamic-update-slice_fusion.6
  9.0 1.7 constant_dynamic-update-slice_fusion.5
  10.7 1.7 constant_dynamic-update-slice_fusion.4
  15.7 18.6 %all-gather.5.cloned.1.call-done = bf16[512,2048]{1,0:T(8,128)(2,1)} async-done(((bf16[512,512]{1,0:T(8,128)(2,1)}), bf16[512,2048]{1,0:T(8,128)(2,1)}) %all-gather.5.cloned.1.call-update) | async-done | bytes 2097168 | tf_op jit(solution)/shard_map/all_gather | solution.py:83
  34.2 2.1 fusion.1
  36.3 201.8 %all-gather.7.cloned.1.call-done = bf16[2048,3584]{1,0:T(8,128)(2,1)} async-done(((bf16[256,3584]{1,0:T(8,128)(2,1)}), bf16[2048,3584]{1,0:T(8,128)(2,1)}) %all-gather.7.cloned.1.call-update) | async-done | bytes 14680080 | tf_op jit(solution)/shard_map/all_gather | solution.py:82
  238.1 11.6 %multiply_convert_fusion = bf16[512,3584]{1,0:T(8,128)(2,1)S(1)} fusion(bf16[2048,3584]{1,0:T(8,128)(2,1)} %all-gather.7.cloned.1.call-done, f32[512]{0:T(512)S(1)} %add_rsqrt_fusion, bf16[512,2048]{1,0:T(8,128)(2,1)} %all-gather.5.cloned.1.call-done, f32[2048]{0:T(1024)S(1)} %copy-done.51), kind=kOutput, calls=%fused_computation.4 | convolution fusion | flops 7523008512 | bytes 20457472 | tf_op jit(solution)/shard_map/dot_general | solution.py:86
  250.0 2.5 collective-permute-start
  252.6 2.5 collective-permute-start.1
  255.1 2.8 convolution_convert_fusion.1
  260.8 1.3 copy.35
  262.1 2.6 convert_multiply_fusion.5
  264.7 2.1 slice.352
  266.8 2.1 slice.353
  268.9 2.1 slice.351
  271.0 2.1 slice.355
  273.0 2.0 multiply_add_fusion.1
  275.0 1.4 slice.358
  276.4 1.4 slice.359
  277.8 1.4 slice.357
  279.1 1.4 slice.361
  280.5 2.0 multiply_add_fusion.2
  283.9 1.6 slice.363
  285.5 1.6 slice.367
  287.1 1.8 multiply_add_fusion.3
  290.2 1.5 slice.369
  291.7 1.5 slice.373
  293.2 1.6 multiply_add_fusion.4
  294.9 1.5 slice.376
  296.3 1.4 slice.377
  297.8 1.5 slice.375
  299.2 1.5 slice.379
  300.7 1.4 multiply_add_fusion.5
  302.1 1.4 slice.382
  303.5 1.4 slice.383
  304.8 1.4 slice.381
  306.2 1.4 slice.385
  307.5 1.4 multiply_add_fusion.6
  310.1 1.3 slice.387
  311.4 1.3 slice.391
  312.8 1.4 multiply_add_fusion.7
  320.1 1.4 fusion.68
  322.1 1.3 slice.386
  326.7 1.4 slice.405
  330.6 1.5 slice.374
  332.1 1.5 slice.407
  336.2 1.5 slice.368
  344.1 1.4 slice.356
  345.5 1.4 slice.413
  348.1 2.1 slice.350
  350.2 2.1 slice.415
  354.7 1.9 fusion.51
  357.8 1.7 pad_maximum_fusion.5
  359.5 2.6 pad.142
  362.1 1.7 pad.143
  363.8 2.9 fusion.39
  367.7 4.6 pad.127
  373.3 26.1 %all-gather.1 = f32[8,1,512]{2,1,0:T(1,128)S(1)} all-gather(f32[1,1,512]{2,1,0:T(1,128)S(1)} %add_bitcast_fusion), channel_id=1, replica_groups=mesh['sp'=8,'tp'=4] {'sp'}, dimensions={0}, use_global_device_ids=true | all-gather | bytes 18432 | tf_op jit(solution)/shard_map/all_gather | solution.py:18
  399.5 2.7 pad.145
  402.3 2.7 pad.144
  405.7 26.1 %all-gather = f32[8,1,512]{2,1,0:T(1,128)S(1)} all-gather(f32[1,1,512]{2,1,0:T(1,128)S(1)} %add_bitcast_fusion.1), channel_id=1, replica_groups=mesh['sp'=8,'tp'=4] {'sp'}, dimensions={0}, use_global_device_ids=true | all-gather | bytes 18432 | tf_op jit(solution)/shard_map/all_gather | solution.py:18
  432.3 5.3 %convolution_convert_fusion = bf16[512,2048]{1,0:T(8,128)(2,1)} fusion(bf16[512,2048]{1,0:T(8,128)(2,1)} %param.39, f32[512,512]{1,0:T(8,128)} %pad.144, f32[512,512]{1,0:T(8,128)} %pad.145, f32[512,512]{1,0:T(8,128)S(1)} %copy-done.10, f32[512,512]{1,0:T(8,128)S(1)} %copy-done.8, bf16[512,3584]{1,0:T(8,128)(2,1)} %copy-done.7, f32[512]{0:T(512)S(1)} %multiply_add_fusion.9), kind=kOutput, calls=%fused_computation.9 | convolution fusion | flops 1078722560 | bytes 8914944 | tf_op jit(solution)/shard_map/dot_general | solution.py:143
  437.7 28.3 %reduce-scatter.5.cloned.1.call-done = bf16[512,512]{1,0:T(8,128)(2,1)} async-done(((bf16[512,2048]{1,0:T(8,128)(2,1)}), bf16[512,512]{1,0:T(8,128)(2,1)}) %reduce-scatter.5.cloned.1.call-update) | async-done | bytes 524304 | tf_op jit(solution)/shard_map/reduce_scatter | solution.py:148
  466.1 2.9 add_convert_fusion
  (248 shorter events, 39.9 us)
Async XLA Ops:
  6.5 248.5 %copy-start = (bf16[512,2048]{1,0:T(8,128)(2,1)S(1)}, bf16[512,2048]{1,0:T(8,128)(2,1)}, u32[]{:S(2)}) copy-start(bf16[512,2048]{1,0:T(8,128)(2,1)} %param.38) | copy-start | bytes 6291460
  6.5 5.9 %copy-start.12 = (bf16[256,512]{1,0:T(8,128)(2,1)S(1)}, bf16[256,512]{1,0:T(8,128)(2,1)}, u32[]{:S(2)}) copy-start(bf16[256,512]{1,0:T(8,128)(2,1)} %param.26) | copy-start | bytes 786436
  6.5 6.6 %copy-start.13 = (bf16[256,512]{1,0:T(8,128)(2,1)S(1)}, bf16[256,512]{1,0:T(8,128)(2,1)}, u32[]{:S(2)}) copy-start(bf16[256,512]{1,0:T(8,128)(2,1)} %param.27) | copy-start | bytes 786436
  6.5 7.4 %copy-start.14 = (bf16[256,512]{1,0:T(8,128)(2,1)S(1)}, bf16[256,512]{1,0:T(8,128)(2,1)}, u32[]{:S(2)}) copy-start(bf16[256,512]{1,0:T(8,128)(2,1)} %param.28) | copy-start | bytes 786436
  6.5 8.1 %copy-start.15 = (bf16[256,512]{1,0:T(8,128)(2,1)S(1)}, bf16[256,512]{1,0:T(8,128)(2,1)}, u32[]{:S(2)}) copy-start(bf16[256,512]{1,0:T(8,128)(2,1)} %param.29) | copy-start | bytes 786436
  6.5 27.7 %all-gather.5.cloned.1.call-start = ((), (), s32[]{:S(2)}) async-start(), calls=%async_computation.2 | async-start | bytes 2621440 | tf_op jit(solution)/shard_map/all_gather | solution.py:83
  7.3 230.9 %all-gather.7.cloned.1.call-start = ((), (), s32[]{:S(2)}) async-start(), calls=%async_computation.3 | async-start | bytes 16515072 | tf_op jit(solution)/shard_map/all_gather | solution.py:82
  12.4 3.2 copy-start.47
  12.4 3.2 copy-start.28
  12.4 3.2 copy-start.25
  15.5 222.7 %copy-start.51 = (f32[2048]{0:T(1024)S(1)}, f32[2048]{0:T(1024)}, u32[]{:S(2)}) copy-start(f32[2048]{0:T(1024)} %param.22) | copy-start | bytes 24580
  15.5 422.3 %reduce-scatter.3.cloned.1.call-start = ((), (), s32[]{:S(2)}) async-start(), calls=%async_computation.4 | async-start | bytes 2621440 | tf_op jit(solution)/shard_map/reduce_scatter | solution.py:145
  249.8 5.3 %copy-start.7 = (bf16[512,3584]{1,0:T(8,128)(2,1)}, bf16[512,3584]{1,0:T(8,128)(2,1)S(1)}, u32[]{:S(2)}) copy-start(bf16[512,3584]{1,0:T(8,128)(2,1)S(1)} %multiply_convert_fusion) | copy-start | bytes 11010052
  250.0 5.1 %collective-permute-start = (f32[2,512]{1,0:T(2,128)S(1)}, f32[2,512]{1,0:T(2,128)S(1)}, u32[]{:S(2)}, u32[]{:S(2)}) collective-permute-start(f32[2,512]{1,0:T(2,128)S(1)} %slice.440), channel_id=1, source_target_pairs={{0,4},{4,8},{8,12},{12,16},{16,20},{20,24},{24,28},{1,5},{5,9},{9,... | collective-permute-start | bytes 12296 | tf_op jit(solution)/shard_map/ppermute | solution.py:13
  252.6 5.5 %collective-permute-start.1 = (f32[3,512]{1,0:T(4,128)S(1)}, f32[3,512]{1,0:T(4,128)S(1)}, u32[]{:S(2)}, u32[]{:S(2)}) collective-permute-start(f32[3,512]{1,0:T(4,128)S(1)} %slice.445), channel_id=1, source_target_pairs={{0,4},{4,8},{8,12},{12,16},{16,20},{20,24},{24,28},{1,5},{5,9},{9,... | collective-permute-start | bytes 18440 | tf_op jit(solution)/shard_map/ppermute | solution.py:13
  257.9 0.9 copy-start.49
  257.9 208.2 %reduce-scatter.5.cloned.1.call-start = ((), (), s32[]{:S(2)}) async-start(), calls=%async_computation.5 | async-start | bytes 2621440 | tf_op jit(solution)/shard_map/reduce_scatter | solution.py:148
  258.6 1.1 copy-start.4
  259.3 1.0 copy-start.50
  260.7 1.3 copy-start.45
  260.8 1.3 copy-start.46
  343.9 8.4 %copy-start.41 = (f32[1,512]{1,0:T(1,128)S(1)}, f32[1,512]{1,0:T(1,128)}, u32[]{:S(2)}) copy-start(f32[1,512]{1,0:T(1,128)} %get-tuple-element.182) | copy-start | bytes 6148
  343.9 8.4 %copy-start.42 = (f32[1,512]{1,0:T(1,128)S(1)}, f32[1,512]{1,0:T(1,128)}, u32[]{:S(2)}) copy-start(f32[1,512]{1,0:T(1,128)} %get-tuple-element.183) | copy-start | bytes 6148
  343.9 8.4 %copy-start.43 = (f32[1,512]{1,0:T(1,128)S(1)}, f32[1,512]{1,0:T(1,128)}, u32[]{:S(2)}) copy-start(f32[1,512]{1,0:T(1,128)} %get-tuple-element.184) | copy-start | bytes 6148
  343.9 8.4 %copy-start.44 = (f32[1,512]{1,0:T(1,128)S(1)}, f32[1,512]{1,0:T(1,128)}, u32[]{:S(2)}) copy-start(f32[1,512]{1,0:T(1,128)} %get-tuple-element.185) | copy-start | bytes 6148
  343.9 8.4 %copy-start.27 = (f32[2,512]{1,0:T(2,128)S(1)}, f32[2,512]{1,0:T(2,128)}, u32[]{:S(2)}) copy-start(f32[2,512]{1,0:T(2,128)} %get-tuple-element.202) | copy-start | bytes 12292
  344.0 8.4 %copy-start.26 = (f32[2,512]{1,0:T(2,128)S(1)}, f32[2,512]{1,0:T(2,128)}, u32[]{:S(2)}) copy-start(f32[2,512]{1,0:T(2,128)} %get-tuple-element.201) | copy-start | bytes 12292
  344.0 8.5 %copy-start.23 = (f32[3,512]{1,0:T(4,128)S(1)}, f32[3,512]{1,0:T(4,128)}, u32[]{:S(2)}) copy-start(f32[3,512]{1,0:T(4,128)} %slice.386) | copy-start | bytes 18436
  344.0 8.5 %copy-start.24 = (f32[3,512]{1,0:T(4,128)S(1)}, f32[3,512]{1,0:T(4,128)}, u32[]{:S(2)}) copy-start(f32[3,512]{1,0:T(4,128)} %slice.403) | copy-start | bytes 18436
  344.0 8.5 %copy-start.40 = (f32[1,512]{1,0:T(1,128)S(1)}, f32[1,512]{1,0:T(1,128)}, u32[]{:S(2)}) copy-start(f32[1,512]{1,0:T(1,128)} %slice.485) | copy-start | bytes 6148
  344.0 8.6 %copy-start.39 = (f32[1,512]{1,0:T(1,128)S(1)}, f32[1,512]{1,0:T(1,128)}, u32[]{:S(2)}) copy-start(f32[1,512]{1,0:T(1,128)} %slice.456) | copy-start | bytes 6148
  344.0 8.6 %copy-start.22 = (f32[7,512]{1,0:T(8,128)S(1)}, f32[7,512]{1,0:T(8,128)}, u32[]{:S(2)}) copy-start(f32[7,512]{1,0:T(8,128)} %slice.405) | copy-start | bytes 43012
  344.0 8.7 %copy-start.38 = (f32[1,512]{1,0:T(1,128)S(1)}, f32[1,512]{1,0:T(1,128)}, u32[]{:S(2)}) copy-start(f32[1,512]{1,0:T(1,128)} %slice.484) | copy-start | bytes 6148
  344.0 8.7 %copy-start.37 = (f32[1,512]{1,0:T(1,128)S(1)}, f32[1,512]{1,0:T(1,128)}, u32[]{:S(2)}) copy-start(f32[1,512]{1,0:T(1,128)} %slice.455) | copy-start | bytes 6148
  344.0 8.8 %copy-start.18 = (f32[15,512]{1,0:T(8,128)S(1)}, f32[15,512]{1,0:T(8,128)}, u32[]{:S(2)}) copy-start(f32[15,512]{1,0:T(8,128)} %slice.374) | copy-start | bytes 92164
  344.0 8.8 %copy-start.19 = (f32[15,512]{1,0:T(8,128)S(1)}, f32[15,512]{1,0:T(8,128)}, u32[]{:S(2)}) copy-start(f32[15,512]{1,0:T(8,128)} %slice.407) | copy-start | bytes 92164
  344.1 8.8 %copy-start.36 = (f32[1,512]{1,0:T(1,128)S(1)}, f32[1,512]{1,0:T(1,128)}, u32[]{:S(2)}) copy-start(f32[1,512]{1,0:T(1,128)} %slice.483) | copy-start | bytes 6148
  345.5 7.5 %copy-start.35 = (f32[1,512]{1,0:T(1,128)S(1)}, f32[1,512]{1,0:T(1,128)}, u32[]{:S(2)}) copy-start(f32[1,512]{1,0:T(1,128)} %slice.454) | copy-start | bytes 6148
  348.1 5.0 %copy-start.16 = (f32[31,512]{1,0:T(8,128)S(1)}, f32[31,512]{1,0:T(8,128)}, u32[]{:S(2)}) copy-start(f32[31,512]{1,0:T(8,128)} %slice.368) | copy-start | bytes 190468
  348.1 5.0 %copy-start.17 = (f32[31,512]{1,0:T(8,128)S(1)}, f32[31,512]{1,0:T(8,128)}, u32[]{:S(2)}) copy-start(f32[31,512]{1,0:T(8,128)} %slice.409) | copy-start | bytes 190468
  350.2 2.9 copy-start.34
  350.2 3.0 copy-start.33
  352.6 0.9 copy-start.11
  352.9 0.7 copy-start.32
  353.1 0.7 copy-start.31
  353.8 2.8 copy-start.30
  354.7 3.1 copy-start.29
  363.7 3.9 copy-start.2
  363.7 3.9 copy-start.3
  367.6 4.7 copy-start.6
  372.4 29.8 %copy-start.5 = (f32[255,512]{1,0:T(8,128)S(1)}, f32[255,512]{1,0:T(8,128)}, u32[]{:S(2)}) copy-start(f32[255,512]{1,0:T(8,128)} %get-tuple-element.157) | copy-start | bytes 1566724
  372.6 26.9 %copy-start.9 = (f32[512,512]{1,0:T(8,128)}, f32[512,512]{1,0:T(8,128)S(1)}, u32[]{:S(2)}) copy-start(f32[512,512]{1,0:T(8,128)S(1)} %pad.126) | copy-start | bytes 3145732
  399.4 32.4 %copy-start.20 = (f32[512]{0:T(512)S(1)}, f32[512]{0:T(512)}, u32[]{:S(2)}) copy-start(f32[512]{0:T(512)} %custom-call) | copy-start | bytes 6148
  399.4 32.4 %copy-start.21 = (f32[512]{0:T(512)S(1)}, f32[512]{0:T(512)}, u32[]{:S(2)}) copy-start(f32[512]{0:T(512)} %custom-call.1) | copy-start | bytes 6148
  399.5 32.9 %copy-start.48 = (f32[512]{0:T(512)S(1)}, f32[512]{0:T(512)}, u32[]{:S(2)}) copy-start(f32[512]{0:T(512)} %param.37) | copy-start | bytes 6148
  399.5 32.9 %copy-start.8 = (f32[512,512]{1,0:T(8,128)S(1)}, f32[512,512]{1,0:T(8,128)}, u32[]{:S(2)}) copy-start(f32[512,512]{1,0:T(8,128)} %pad.127) | copy-start | bytes 3145732
  402.2 30.1 %copy-start.10 = (f32[512,512]{1,0:T(8,128)S(1)}, f32[512,512]{1,0:T(8,128)}, u32[]{:S(2)}) copy-start(f32[512,512]{1,0:T(8,128)} %copy-done.9) | copy-start | bytes 3145732
  437.7 31.3 %copy-start.1 = (bf16[512,2048]{1,0:T(8,128)(2,1)S(1)}, bf16[512,2048]{1,0:T(8,128)(2,1)}, u32[]{:S(2)}) copy-start(bf16[512,2048]{1,0:T(8,128)(2,1)} %param.38) | copy-start | bytes 6291460
Sparse Core Ops, SparseCore 0:
  8.9 25.2 all-gather.4
  36.4 201.6 all-gather.6
  258.0 30.6 reduce-scatter.2
  437.8 28.1 reduce-scatter.4
where the time goes:
time: 478 us; the launch traced here: 476 us
  waiting for transfers between devices  249 us (52%)
  local copies, waits for them, and re-layouts  100 us (21%)
  blocking collectives  52.2 us (11%)
  other arithmetic  33 us (7%)
  matrix products  20.7 us (4%)
  between operations  14.2 us (3%)
  starting transfers between devices  5.26 us (1%)
    all_gather x1, waiting for transfers between devices, local(): whole_weight = lax.all_gather(local_cat, 'sp', axis=0, tiled=True)  202 us
    slice x60, local copies, waits for them, and re-layouts, local(): lax.associative_scan(linear_chain, (decay, drive), axis=0)  73.1 us
    all_gather x2, blocking collectives, entering(): everything = jax.tree.map(lambda part: lax.all_gather(part, axis), value)  52.2 us
    reduce_scatter x1, waiting for transfers between devices, local(): lax.psum_scatter(lru_part.astype(jnp.bfloat16), 'tp', scatter_dimension=1...  28.3 us
    all_gather x1, waiting for transfers between devices, local(): piece = lax.all_gather(sequence_activations, 'tp', axis=1, tiled=True)  18.6 us
    add x16, other arithmetic, linear_chain(): return (earlier[0] * later[0], later[0] * earlier[1] + later[1])  17.2 us
    pad x32, local copies, waits for them, and re-layouts, local(): lax.associative_scan(linear_chain, (decay, drive), axis=0)  16 us
    dot_general x1, matrix products, local(): jnp.dot(scaled_piece, whole_weight, preferred_element_type=jnp.float32)  11.6 us
  transfers between devices with their start and end apart: 6, of which 3 were waited for; matrix products, arithmetic and copies ran while one was open for 29% of the time, Pallas kernels for 0%

commit v1 on v0

--- a/solution.py
+++ b/solution.py
@@ -2,6 +2,7 @@
 import jax.numpy as jnp
 from jax import lax
 from jax.sharding import PartitionSpec as P
+from jax.lax import axis_index, axis_size, ppermute
 
 scan_switch_exponent = 8.0
 norm_eps = 1e-06
@@ -79,7 +80,23 @@
         scan_blend_matrix,
     ]
     local_cat = jnp.concatenate(pieces, axis=1)
-    whole_weight = lax.all_gather(local_cat, "sp", axis=0, tiled=True)
+
+    def sides_switch(w_in):
+        chip_axis = "sp"
+        degree = axis_size(chip_axis)
+        block_next = range(degree)
+        p_next = map(lambda q: (q, (q + 1) % degree), block_next)
+        tray = list(p_next)
+        block_out = [None] * degree
+        block_out[degree - 1] = w_in
+        for nth in range(degree - 2, -1, -1):
+            block_out[nth] = ppermute(block_out[nth + 1], chip_axis, tray)
+        base_arr = jnp.concatenate(block_out, 0)
+        outcome_arr = axis_index(chip_axis)
+        y2 = (outcome_arr + 1) * w_in.shape[0]
+        return jnp.roll(base_arr, y2, axis=0)
+
+    whole_weight = sides_switch(local_cat)
     piece = lax.all_gather(sequence_activations, "tp", axis=1, tiled=True)
     piece_float = piece.astype(jnp.float32)
     scaled_piece = (piece.astype(jnp.float32) * entry_rescale_vector[None, :]).astype(jnp.bfloat16)

time: 478 us -> 658 us (1.38)
  local copies, waits for them, and re-layouts: 100 us -> 181 us
  waiting for transfers between devices: 249 us -> 317 us
  other arithmetic: 33 us -> 60.9 us
    ppermute x0 -> x7, waiting for transfers between devices: none -> 289 us  [sides_switch(): block_out[nth] = ppermute(block_out[nth + 1], chip_axis, tray)]
    all_gather x1 -> x0, waiting for transfers between devices: 202 us -> none  [local(): whole_weight = lax.all_gather(local_cat, 'sp', axis=0, tiled=True)]
    unnamed x112 -> x83, local copies, waits for them, and re-layouts: 8.6 us -> 55.8 us
    all_gather x1, waiting for transfers between devices: 18.6 us -> 0.02 us  [local(): piece = lax.all_gather(sequence_activations, 'tp', axis=1, tiled=True)]
    pad x32, local copies, waits for them, and re-layouts: 16 us -> 33.4 us  [local(): lax.associative_scan(linear_chain, (decay, drive), axis=0)]
    slice x60, local copies, waits for them, and re-layouts: 73.1 us -> 86.8 us  [local(): lax.associative_scan(linear_chain, (decay, drive), axis=0)]
    concatenate x15, other arithmetic: 1.95 us -> 11.3 us  [local(): lax.associative_scan(linear_chain, (decay, drive), axis=0)]
    add x15, other arithmetic: 2.5 us -> 10.4 us  [local(): lax.associative_scan(linear_chain, (decay, drive), axis=0)]
  transfers between devices with their start and end apart: 6 -> 12, of which waited for: 3 -> 8; matrix products, arithmetic and copies ran while one was open for 29% -> 29% of each run, Pallas kernels for 0% -> 0%
where the time goes in v1:
time: 658 us; the launch traced here: 653 us
  waiting for transfers between devices  317 us (48%)
  local copies, waits for them, and re-layouts  181 us (28%)
  other arithmetic  60.9 us (9%)
  blocking collectives  52.2 us (8%)
  matrix products  22.9 us (3%)
  between operations  13.6 us (2%)
    ppermute x7, waiting for transfers between devices, sides_switch(): block_out[nth] = ppermute(block_out[nth + 1], chip_axis, tray)  289 us
    slice x60, local copies, waits for them, and re-layouts, local(): lax.associative_scan(linear_chain, (decay, drive), axis=0)  86.8 us
    unnamed x83, local copies, waits for them, and re-layouts  55.8 us
    all_gather x2, blocking collectives, entering(): everything = jax.tree.map(lambda part: lax.all_gather(part, axis), value)  52.2 us
    pad x32, local copies, waits for them, and re-layouts, local(): lax.associative_scan(linear_chain, (decay, drive), axis=0)  33.4 us
    reduce_scatter x1, waiting for transfers between devices, local(): lax.psum_scatter(lru_part.astype(jnp.bfloat16), 'tp', scatter_dimension=1...  27.6 us
    add x16, other arithmetic, linear_chain(): return (earlier[0] * later[0], later[0] * earlier[1] + later[1])  23.6 us
  transfers between devices with their start and end apart: 12, of which 8 were waited for; matrix products, arithmetic and copies ran while one was open for 29% of the time, Pallas kernels for 0%

profile of v1, /device:TPU:0, one launch (start us, length us, event | category | flops | bytes accessed | tf_op | source)
XLA Modules:
  0.0 653.4 jit_solution(411651596755064644)
XLA Ops:
  13.6 3.0 collective-permute-start
  16.6 43.0 %collective-permute-done = bf16[256,3584]{1,0:T(8,128)(2,1)S(1)} collective-permute-done((bf16[256,3584]{1,0:T(8,128)(2,1)S(1)}, bf16[256,3584]{1,0:T(8,128)(2,1)S(1)}, u32[]{:S(2)}, u32[]{:S(2)}) %collective-permute-start) | collective-permute-done | bytes 1835040 | tf_op jit(solution)/shard_map/ppermute | solution.py:93
  60.9 43.9 %collective-permute-done.1 = bf16[256,3584]{1,0:T(8,128)(2,1)S(1)} collective-permute-done((bf16[256,3584]{1,0:T(8,128)(2,1)S(1)}, bf16[256,3584]{1,0:T(8,128)(2,1)S(1)}, u32[]{:S(2)}, u32[]{:S(2)}) %collective-permute-start.1) | collective-permute-done | bytes 1835040 | tf_op jit(solution)/shard_map/ppermute | solution.py:93
  106.0 43.0 %collective-permute-done.2 = bf16[256,3584]{1,0:T(8,128)(2,1)S(1)} collective-permute-done((bf16[256,3584]{1,0:T(8,128)(2,1)S(1)}, bf16[256,3584]{1,0:T(8,128)(2,1)S(1)}, u32[]{:S(2)}, u32[]{:S(2)}) %collective-permute-start.2) | collective-permute-done | bytes 1835040 | tf_op jit(solution)/shard_map/ppermute | solution.py:93
  150.3 42.2 %collective-permute-done.3 = bf16[256,3584]{1,0:T(8,128)(2,1)S(1)} collective-permute-done((bf16[256,3584]{1,0:T(8,128)(2,1)S(1)}, bf16[256,3584]{1,0:T(8,128)(2,1)S(1)}, u32[]{:S(2)}, u32[]{:S(2)}) %collective-permute-start.3) | collective-permute-done | bytes 1835040 | tf_op jit(solution)/shard_map/ppermute | solution.py:93
  193.7 41.4 %collective-permute-done.4 = bf16[256,3584]{1,0:T(8,128)(2,1)} collective-permute-done((bf16[256,3584]{1,0:T(8,128)(2,1)S(1)}, bf16[256,3584]{1,0:T(8,128)(2,1)}, u32[]{:S(2)}, u32[]{:S(2)}) %collective-permute-start.4) | collective-permute-done | bytes 1835040 | tf_op jit(solution)/shard_map/ppermute | solution.py:93
  235.2 40.7 %collective-permute-done.5 = bf16[256,3584]{1,0:T(8,128)(2,1)} collective-permute-done((bf16[256,3584]{1,0:T(8,128)(2,1)}, bf16[256,3584]{1,0:T(8,128)(2,1)}, u32[]{:S(2)}, u32[]{:S(2)}) %collective-permute-start.5) | collective-permute-done | bytes 1835040 | tf_op jit(solution)/shard_map/ppermute | solution.py:93
  278.3 2.2 fusion.5
  280.6 35.2 %collective-permute-done.6 = bf16[256,3584]{1,0:T(8,128)(2,1)} collective-permute-done((bf16[256,3584]{1,0:T(8,128)(2,1)}, bf16[256,3584]{1,0:T(8,128)(2,1)}, u32[]{:S(2)}, u32[]{:S(2)}) %collective-permute-start.6) | collective-permute-done | bytes 1835040 | tf_op jit(solution)/shard_map/ppermute | solution.py:93
  315.8 2.9 constant_dynamic-update-slice_fusion.22
  318.7 2.8 constant_dynamic-update-slice_fusion.21
  321.5 2.9 constant_dynamic-update-slice_fusion.20
  324.4 2.9 constant_dynamic-update-slice_fusion.19
  327.3 2.9 constant_dynamic-update-slice_fusion.18
  330.2 2.9 constant_dynamic-update-slice_fusion.17
  333.0 2.9 constant_dynamic-update-slice_fusion.16
  341.2 2.8 constant_dynamic-update-slice_fusion.14
  344.1 2.9 constant_dynamic-update-slice_fusion.13
  346.9 2.9 constant_dynamic-update-slice_fusion.12
  360.6 11.1 %multiply_convert_fusion = bf16[512,3584]{1,0:T(8,128)(2,1)S(1)} fusion(bf16[4096,3584]{1,0:T(8,128)(2,1)} %constant_dynamic-update-slice_fusion.23, s32[]{:T(128)S(6)} %select_n.53, f32[512]{0:T(512)S(1)} %add_rsqrt_fusion, bf16[512,2048]{1,0:T(8,128)(2,1)S(1)} %copy-done.16, f32[2048]{0:T(1024)S(1)} %copy-done.23), kind=kOutput, calls=%fused_computation.6 | convolution fusion | flops 7523008512 | bytes 20457476 | tf_op jit(solution)/shard_map/dot_general | solution.py:103
  374.6 2.8 convolution_convert_fusion.1
  381.8 1.6 fusion.13
  384.7 3.7 convert_multiply_fusion.5
  388.4 2.1 slice.415
  390.6 2.1 slice.353
  392.6 3.7 slice.350
  396.4 3.7 slice.351
  400.0 2.1 slice.352
  402.1 3.7 slice.355
  405.7 2.7 multiply_add_fusion.1
  408.5 2.5 slice.359
  411.0 2.5 slice.358
  413.4 2.5 slice.357
  415.9 2.5 slice.361
  418.4 2.0 multiply_add_fusion.2
  420.4 1.6 slice.411
  422.1 1.6 slice.365
  425.1 1.6 slice.364
  427.4 1.8 multiply_add_fusion.3
  433.6 1.6 multiply_add_fusion.4
  482.4 2.5 slice.413
  484.9 2.5 slice.356
  504.8 2.2 pad.138
  509.2 1.8 fusion.56
  511.7 2.4 pad.123
  514.1 1.7 add.340
  515.8 2.6 pad.125
  518.4 2.4 pad.141
  523.1 1.8 add.351
  524.9 2.1 fusion.55
  527.1 1.8 pad.124
  528.9 2.6 pad.143
  532.5 1.7 pad.142
  534.2 3.0 fusion.43
  537.9 2.1 add.352
  541.3 2.9 pad.144
  544.2 4.7 pad.145
  550.0 2.8 pad.126
  552.7 2.7 pad.127
  556.2 26.1 %all-gather = f32[8,1,512]{2,1,0:T(1,128)S(1)} all-gather(f32[1,1,512]{2,1,0:T(1,128)S(1)} %add_bitcast_fusion.1), channel_id=1, replica_groups=mesh['sp'=8,'tp'=4] {'sp'}, dimensions={0}, use_global_device_ids=true | all-gather | bytes 18432 | tf_op jit(solution)/shard_map/all_gather | solution.py:19
  583.1 26.1 %all-gather.1 = f32[8,1,512]{2,1,0:T(1,128)S(1)} all-gather(f32[1,1,512]{2,1,0:T(1,128)S(1)} %add_bitcast_fusion), channel_id=1, replica_groups=mesh['sp'=8,'tp'=4] {'sp'}, dimensions={0}, use_global_device_ids=true | all-gather | bytes 18432 | tf_op jit(solution)/shard_map/all_gather | solution.py:19
  610.3 6.0 convolution_convert_fusion
  616.4 27.6 %reduce-scatter.5.cloned.1.call-done = bf16[512,512]{1,0:T(8,128)(2,1)} async-done(((bf16[512,2048]{1,0:T(8,128)(2,1)}), bf16[512,512]{1,0:T(8,128)(2,1)}) %reduce-scatter.5.cloned.1.call-update) | async-done | bytes 524304 | tf_op jit(solution)/shard_map/reduce_scatter | solution.py:165
  644.0 2.9 add_convert_fusion
  (231 shorter events, 122.3 us)
Async XLA Ops:
  6.5 368.1 %copy-start = (bf16[512,2048]{1,0:T(8,128)(2,1)S(1)}, bf16[512,2048]{1,0:T(8,128)(2,1)}, u32[]{:S(2)}) copy-start(bf16[512,2048]{1,0:T(8,128)(2,1)} %param.38) | copy-start | bytes 6291460
  6.5 329.4 %copy-start.9 = (bf16[256,512]{1,0:T(8,128)(2,1)S(1)}, bf16[256,512]{1,0:T(8,128)(2,1)}, u32[]{:S(2)}) copy-start(bf16[256,512]{1,0:T(8,128)(2,1)} %param.23) | copy-start | bytes 786436
  6.5 330.2 %copy-start.10 = (bf16[256,512]{1,0:T(8,128)(2,1)S(1)}, bf16[256,512]{1,0:T(8,128)(2,1)}, u32[]{:S(2)}) copy-start(bf16[256,512]{1,0:T(8,128)(2,1)} %param.24) | copy-start | bytes 786436
  6.5 330.9 %copy-start.11 = (bf16[256,512]{1,0:T(8,128)(2,1)S(1)}, bf16[256,512]{1,0:T(8,128)(2,1)}, u32[]{:S(2)}) copy-start(bf16[256,512]{1,0:T(8,128)(2,1)} %param.25) | copy-start | bytes 786436
  6.5 331.7 %copy-start.12 = (bf16[256,512]{1,0:T(8,128)(2,1)S(1)}, bf16[256,512]{1,0:T(8,128)(2,1)}, u32[]{:S(2)}) copy-start(bf16[256,512]{1,0:T(8,128)(2,1)} %param.26) | copy-start | bytes 786436
  6.6 332.4 %copy-start.13 = (bf16[256,512]{1,0:T(8,128)(2,1)S(1)}, bf16[256,512]{1,0:T(8,128)(2,1)}, u32[]{:S(2)}) copy-start(bf16[256,512]{1,0:T(8,128)(2,1)} %param.27) | copy-start | bytes 786436
  6.6 271.7 %all-gather.4.cloned.1.call-start = ((), (), s32[]{:S(2)}) async-start(), calls=%async_computation.2 | async-start | bytes 2621440 | tf_op jit(solution)/shard_map/all_gather | solution.py:100
  13.6 46.1 %collective-permute-start = (bf16[256,3584]{1,0:T(8,128)(2,1)S(1)}, bf16[256,3584]{1,0:T(8,128)(2,1)S(1)}, u32[]{:S(2)}, u32[]{:S(2)}) collective-permute-start(bf16[256,3584]{1,0:T(8,128)(2,1)S(1)} %constant_dynamic-update-slice_fusion), channel_id=1, source_target_pairs={{0,4},{4,8},{8,12},{12,16},{16,20},{20,24},{24,28},{28,0},{1,5},{5... | collective-permute-start | bytes 5505032 | tf_op jit(solution)/shard_map/ppermute | solution.py:93
  59.6 1.3 copy-start.1
  60.9 43.9 %collective-permute-start.1 = (bf16[256,3584]{1,0:T(8,128)(2,1)S(1)}, bf16[256,3584]{1,0:T(8,128)(2,1)S(1)}, u32[]{:S(2)}, u32[]{:S(2)}) collective-permute-start(bf16[256,3584]{1,0:T(8,128)(2,1)S(1)} %collective-permute-done), channel_id=1, source_target_pairs={{0,4},{4,8},{8,12},{12,16},{16,20},{20,24},{24,28},{28,0},{1,5},{5... | collective-permute-start | bytes 5505032 | tf_op jit(solution)/shard_map/ppermute | solution.py:93
  104.8 1.2 copy-start.3
  106.0 43.0 %collective-permute-start.2 = (bf16[256,3584]{1,0:T(8,128)(2,1)S(1)}, bf16[256,3584]{1,0:T(8,128)(2,1)S(1)}, u32[]{:S(2)}, u32[]{:S(2)}) collective-permute-start(bf16[256,3584]{1,0:T(8,128)(2,1)S(1)} %collective-permute-done.1), channel_id=1, source_target_pairs={{0,4},{4,8},{8,12},{12,16},{16,20},{20,24},{24,28},{28,0},{1,5},{5... | collective-permute-start | bytes 5505032 | tf_op jit(solution)/shard_map/ppermute | solution.py:93
  149.0 1.3 copy-start.5
  150.3 42.2 %collective-permute-start.3 = (bf16[256,3584]{1,0:T(8,128)(2,1)S(1)}, bf16[256,3584]{1,0:T(8,128)(2,1)S(1)}, u32[]{:S(2)}, u32[]{:S(2)}) collective-permute-start(bf16[256,3584]{1,0:T(8,128)(2,1)S(1)} %collective-permute-done.2), channel_id=1, source_target_pairs={{0,4},{4,8},{8,12},{12,16},{16,20},{20,24},{24,28},{28,0},{1,5},{5... | collective-permute-start | bytes 5505032 | tf_op jit(solution)/shard_map/ppermute | solution.py:93
  192.5 1.2 copy-start.7
  193.7 41.4 %collective-permute-start.4 = (bf16[256,3584]{1,0:T(8,128)(2,1)S(1)}, bf16[256,3584]{1,0:T(8,128)(2,1)}, u32[]{:S(2)}, u32[]{:S(2)}) collective-permute-start(bf16[256,3584]{1,0:T(8,128)(2,1)S(1)} %collective-permute-done.3), channel_id=1, source_target_pairs={{0,4},{4,8},{8,12},{12,16},{16,20},{20,24},{24,28},{28,0},{1,5},{5... | collective-permute-start | bytes 5505032 | tf_op jit(solution)/shard_map/ppermute | solution.py:93
  235.1 40.8 %collective-permute-start.5 = (bf16[256,3584]{1,0:T(8,128)(2,1)}, bf16[256,3584]{1,0:T(8,128)(2,1)}, u32[]{:S(2)}, u32[]{:S(2)}) collective-permute-start(bf16[256,3584]{1,0:T(8,128)(2,1)} %collective-permute-done.4), channel_id=1, source_target_pairs={{0,4},{4,8},{8,12},{12,16},{16,20},{20,24},{24,28},{28,0},{1,5},{5... | collective-permute-start | bytes 5505032 | tf_op jit(solution)/shard_map/ppermute | solution.py:93
  235.1 381.2 %reduce-scatter.3.cloned.1.call-start = ((), (), s32[]{:S(2)}) async-start(), calls=%async_computation.3 | async-start | bytes 2621440 | tf_op jit(solution)/shard_map/reduce_scatter | solution.py:162
  275.9 39.9 %collective-permute-start.6 = (bf16[256,3584]{1,0:T(8,128)(2,1)}, bf16[256,3584]{1,0:T(8,128)(2,1)}, u32[]{:S(2)}, u32[]{:S(2)}) collective-permute-start(bf16[256,3584]{1,0:T(8,128)(2,1)} %collective-permute-done.5), channel_id=1, source_target_pairs={{0,4},{4,8},{8,12},{12,16},{16,20},{20,24},{24,28},{28,0},{1,5},{5... | collective-permute-start | bytes 5505032 | tf_op jit(solution)/shard_map/ppermute | solution.py:93
  278.3 61.4 %copy-start.14 = (bf16[256,512]{1,0:T(8,128)(2,1)S(1)}, bf16[256,512]{1,0:T(8,128)(2,1)}, u32[]{:S(2)}) copy-start(bf16[256,512]{1,0:T(8,128)(2,1)} %param.28) | copy-start | bytes 786436
  278.3 62.2 %copy-start.15 = (bf16[256,512]{1,0:T(8,128)(2,1)S(1)}, bf16[256,512]{1,0:T(8,128)(2,1)}, u32[]{:S(2)}) copy-start(bf16[256,512]{1,0:T(8,128)(2,1)} %param.29) | copy-start | bytes 786436
  278.3 71.5 %copy-start.8 = (bf16[256,3584]{1,0:T(8,128)(2,1)S(1)}, bf16[256,3584]{1,0:T(8,128)(2,1)}, u32[]{:S(2)}) copy-start(bf16[256,3584]{1,0:T(8,128)(2,1)} %copy-done.7) | copy-start | bytes 5505028
  278.3 72.9 %copy-start.6 = (bf16[256,3584]{1,0:T(8,128)(2,1)S(1)}, bf16[256,3584]{1,0:T(8,128)(2,1)}, u32[]{:S(2)}) copy-start(bf16[256,3584]{1,0:T(8,128)(2,1)} %copy-done.5) | copy-start | bytes 5505028
  278.3 74.2 %copy-start.4 = (bf16[256,3584]{1,0:T(8,128)(2,1)S(1)}, bf16[256,3584]{1,0:T(8,128)(2,1)}, u32[]{:S(2)}) copy-start(bf16[256,3584]{1,0:T(8,128)(2,1)} %copy-done.3) | copy-start | bytes 5505028
  278.3 75.7 %copy-start.2 = (bf16[256,3584]{1,0:T(8,128)(2,1)S(1)}, bf16[256,3584]{1,0:T(8,128)(2,1)}, u32[]{:S(2)}) copy-start(bf16[256,3584]{1,0:T(8,128)(2,1)} %copy-done.1) | copy-start | bytes 5505028
  280.6 80.0 %copy-start.16 = (bf16[512,2048]{1,0:T(8,128)(2,1)S(1)}, bf16[512,2048]{1,0:T(8,128)(2,1)}, u32[]{:S(2)}) copy-start(bf16[512,2048]{1,0:T(8,128)(2,1)} %all-gather.4.cloned.1.call-done) | copy-start | bytes 6291460
  280.6 80.0 %copy-start.23 = (f32[2048]{0:T(1024)S(1)}, f32[2048]{0:T(1024)}, u32[]{:S(2)}) copy-start(f32[2048]{0:T(1024)} %param.22) | copy-start | bytes 24580
  371.7 2.9 copy-start.18
  371.7 13.0 %copy-start.21 = (f32[512]{0:T(512)S(1)}, f32[512]{0:T(512)}, u32[]{:S(2)}) copy-start(f32[512]{0:T(512)} %param.36) | copy-start | bytes 6148
  371.7 13.0 %copy-start.22 = (f32[512]{0:T(512)S(1)}, f32[512]{0:T(512)}, u32[]{:S(2)}) copy-start(f32[512]{0:T(512)} %param.35) | copy-start | bytes 6148
  371.9 2.7 collective-permute-start.7
  373.3 4.4 collective-permute-start.8
  377.4 266.6 %reduce-scatter.5.cloned.1.call-start = ((), (), s32[]{:S(2)}) async-start(), calls=%async_computation.4 | async-start | bytes 2621440 | tf_op jit(solution)/shard_map/reduce_scatter | solution.py:165
  378.2 0.8 copy-start.17
  471.8 137.3 %copy-start.19 = (f32[512]{0:T(512)S(1)}, f32[512]{0:T(512)}, u32[]{:S(2)}) copy-start(f32[512]{0:T(512)} %custom-call) | copy-start | bytes 6148
  471.8 137.3 %copy-start.20 = (f32[512]{0:T(512)S(1)}, f32[512]{0:T(512)}, u32[]{:S(2)}) copy-start(f32[512]{0:T(512)} %custom-call.1) | copy-start | bytes 6148
Sparse Core Ops, SparseCore 0:
  235.3 23.2 all-gather.3
  377.6 29.7 reduce-scatter.2
  616.5 27.4 reduce-scatter.4
